TPU v7x, 32 devices: a whole 2x2x4 slice. The times are simulated.
32 devices in a mesh: sp: 8 (over z, x), dp: 4 (over y, core).
Axes of the slice: x: 2, y: 2, z: 4, core: 2. Of those that a mesh axis runs over, the one named last changes fastest.
Arguments:
- queries: bfloat16 [4, 1024, 2048], P('dp', 'sp'), may hold values from -6 to 6
- keys: bfloat16 [4, 1024, 2048], P('dp', 'sp'), may hold values from -6 to 6
- values: bfloat16 [4, 1024, 2048], P('dp', 'sp'), may hold values from -6 to 6
- gate_totals: float32 [4, 1024, 32], P('dp', 'sp'), may hold values from -1024 to 0, as said below
- w_out: bfloat16 [2048, 2048], P(None, 'dp'), may hold values from -1 to 1
Outputs:
- mixed: bfloat16 [4, 1024, 2048], P('dp', 'sp')
Inputs may be any that keep to these rules, and one draw needn't show every extreme that they name: `gate_totals`: never rising along a sequence.
All inputs are finite; a program needn't handle non-finite values.
Results may differ from a plain program's by a relative error of at most 0.0053.
Values may be sent and summed in bfloat16 or wider, within the bound.
A program may use at most 64 MiB of HBM per device.

v0:
```python
import jax
import jax.numpy as jnp
from jax import lax
from jax.sharding import PartitionSpec as P

HEAD_DIM = 64


def attend(queries, key_rows, value_rows, totals):
    length = queries.shape[0]
    block_rows = min(length, 512)
    pieces = []
    for begin_row in range(0, length, block_rows):
        end_row = begin_row + block_rows
        scaled = queries[begin_row:end_row] * jnp.bfloat16(HEAD_DIM ** (-0.5))
        scores = jnp.einsum(
            "qhd,khd->hqk", scaled, key_rows[:end_row], preferred_element_type=jnp.float32
        )
        causal = jnp.arange(end_row)[None, :] <= (begin_row + jnp.arange(block_rows))[:, None]
        scores = jnp.where(
            causal[None],
            scores
            + jnp.transpose(totals[begin_row:end_row])[:, :, None]
            - jnp.transpose(totals[:end_row])[:, None, :],
            -jnp.inf,
        )
        biggest = jnp.max(scores, axis=-1, keepdims=True)
        expo = jnp.exp(scores - biggest)
        summed = jnp.sum(expo, axis=-1)
        weights = expo.astype(jnp.bfloat16)
        output = jnp.einsum(
            "hqk,khd->qhd", weights, value_rows[:end_row], preferred_element_type=jnp.float32
        )
        output = output / jnp.transpose(summed)[:, :, None]
        pieces.append(output.astype(jnp.bfloat16))
    return jnp.concatenate(pieces, axis=0).reshape(length, -1)


def local(queries, keys, values, gate_totals, w_out):
    moved = (
        lax.all_to_all(queries, "sp", split_axis=2, concat_axis=1, tiled=True),
        lax.all_to_all(keys, "sp", split_axis=2, concat_axis=1, tiled=True),
        lax.all_to_all(values, "sp", split_axis=2, concat_axis=1, tiled=True),
    )
    totals = lax.all_to_all(gate_totals, "sp", split_axis=2, concat_axis=1, tiled=True)
    held, length = (moved[0].shape[0], moved[0].shape[1])
    query_heads, key_heads, value_heads = [
        part_array[0].reshape(length, -1, HEAD_DIM) for part_array in moved
    ]
    outputs = [attend(query_heads, key_heads, value_heads, totals[0])]
    attended = jnp.stack(outputs, axis=0)
    local_rows = lax.all_to_all(attended, "sp", split_axis=1, concat_axis=2, tiled=True)
    flat_rows = local_rows.reshape(-1, local_rows.shape[2])
    mixed = jnp.dot(
        flat_rows,
        lax.all_gather(w_out, "dp", axis=1, tiled=True),
        preferred_element_type=jnp.float32,
    )
    return mixed.astype(jnp.bfloat16).reshape(local_rows.shape[0], local_rows.shape[1], -1)


def solution(mesh):
    placed = (
        P("dp", "sp", None),
        P("dp", "sp", None),
        P("dp", "sp", None),
        P("dp", "sp", None),
        P(None, "dp"),
    )
    return jax.shard_map(
        local, mesh=mesh, in_specs=placed, out_specs=P("dp", "sp", None), check_vma=False
    )
```

profile of v0, /device:TPU:0, one launch (start us, length us, event | category | flops | bytes accessed | tf_op | source)
XLA Modules:
  0.0 138.5 jit_solution(7458643636415226542)
XLA Ops:
  6.5 0.0 all-gather.2.cloned.1.call-start
  6.5 0.7 all-gather.2.cloned.1.call-update
  7.3 7.3 %all-to-all-start.2 = ((f32[1,128,32]{1,0,2:T(1,128)}), f32[1,128,32]{1,0,2:T(1,128)S(1)}, u32[]{:S(2)}, u32[]{:S(2)}) async-start(f32[1,128,32]{1,0,2:T(1,128)} %bitcast.98), calls=%async_computation.2 | async-start | bytes 32768 | tf_op jit(solution)/shard_map/all_to_all | solution.py:45
  14.6 2.3 %copy.32 = bf16[1,128,2048]{1,0,2:T(2,128)(2,1)S(1)} copy(bf16[1,128,2048]{2,1,0:T(8,128)(2,1)} %param.6) | data formatting | bytes 1048576 | tf_op args[1]
  16.9 0.6 broadcast.36
  17.5 11.6 %reduce.2 = bf16[2048,128]{1,0:T(8,128)(2,1)S(1)} reduce(bf16[2048,1,128]{2,1,0:T(2,128)(2,1)S(1)} %bitcast.83, bf16[]{:T(256)} %broadcast.36), dimensions={1}, to_apply=%bitcast.66.reduce_sub_computation | reduce | bytes 1048578
  29.0 1.0 reshape.70
  30.0 0.0 all-to-all-done.2
  30.0 6.0 %all-to-all-start.1 = ((bf16[8,2,16384]{2,1,0:T(2,128)(2,1)}), bf16[8,2,16384]{2,1,0:T(2,128)(2,1)S(1)}, u32[]{:S(2)}, u32[]{:S(2)}) async-start(bf16[8,2,16384]{2,1,0:T(2,128)(2,1)} %reshape.70), calls=%async_computation.1 | async-start | bytes 1048576 | tf_op jit(solution)/shard_map/all_to_all | solution.py:42
  36.0 0.0 copy-done.2
  36.0 0.8 copy.35
  36.8 11.5 %reduce = bf16[2048,128]{1,0:T(8,128)(2,1)S(1)} reduce(bf16[2048,1,128]{2,1,0:T(2,128)(2,1)S(1)} %bitcast.85, bf16[]{:T(256)} %broadcast.36), dimensions={1}, to_apply=%bitcast.62.reduce_sub_computation | reduce | bytes 1048578
  48.3 0.9 reshape.66
  49.2 0.8 all-to-all-done.1
  50.0 5.2 %all-to-all-start.3 = ((bf16[8,2,16384]{2,1,0:T(2,128)(2,1)}), bf16[8,2,16384]{2,1,0:T(2,128)(2,1)S(1)}, u32[]{:S(2)}, u32[]{:S(2)}) async-start(bf16[8,2,16384]{2,1,0:T(2,128)(2,1)} %reshape.66), calls=%async_computation.3 | async-start | bytes 1048576 | tf_op jit(solution)/shard_map/all_to_all | solution.py:43
  55.2 0.0 copy-done.3
  55.2 0.8 copy.30
  56.0 11.5 %reduce.1 = bf16[2048,128]{1,0:T(8,128)(2,1)S(1)} reduce(bf16[2048,1,128]{2,1,0:T(2,128)(2,1)S(1)} %bitcast.86, bf16[]{:T(256)} %broadcast.36), dimensions={1}, to_apply=%bitcast.64.reduce_sub_computation | reduce | bytes 1048578
  67.5 1.0 reshape.68
  68.5 0.1 all-to-all-done.3
  68.6 5.9 %all-to-all-start = ((bf16[8,2,16384]{2,1,0:T(2,128)(2,1)}), bf16[8,2,16384]{2,1,0:T(2,128)(2,1)S(1)}, u32[]{:S(2)}, u32[]{:S(2)}) async-start(bf16[8,2,16384]{2,1,0:T(2,128)(2,1)} %reshape.68), calls=%async_computation | async-start | bytes 1048576 | tf_op jit(solution)/shard_map/all_to_all | solution.py:41
  74.5 0.1 iota_compare_fusion.1
  74.5 0.4 iota_compare_fusion
  74.9 0.5 reshape.71
  75.5 0.1 copy.46
  75.5 0.3 copy.39
  75.9 0.7 slice.45
  76.6 0.5 reshape.67
  77.2 0.1 copy.44
  77.2 0.3 copy.40
  77.6 0.7 slice.43
  78.3 8.9 %all-to-all-done = bf16[8,2,16384]{2,1,0:T(2,128)(2,1)S(1)} async-done(((bf16[8,2,16384]{2,1,0:T(2,128)(2,1)}), bf16[8,2,16384]{2,1,0:T(2,128)(2,1)S(1)}, u32[]{:S(2)}, u32[]{:S(2)}) %all-to-all-start) | async-done | bytes 524320 | tf_op jit(solution)/shard_map/all_to_all | solution.py:41
  87.2 0.5 reshape.69
  87.8 0.0 copy-start
  87.8 0.0 copy-start.1
  87.8 0.1 copy.45
  87.9 0.2 copy.38
  88.1 0.8 mul.15
  89.0 1.0 reshape_squeeze.7
  90.0 0.2 reshape_squeeze.8
  90.2 0.2 copy.31
  90.4 0.1 mul.13
  90.5 0.2 copy.33
  90.7 0.1 slice.35
  90.9 0.2 copy.36
  91.1 0.1 slice.39
  91.2 1.2 fusion.8
  92.3 1.2 fusion.6
  93.6 0.0 copy-start.4
  93.6 1.4 %fusion.22 = bf16[512,4,64]{0,2,1:T(8,128)(2,1)S(1)} fusion(bf16[512,4,64]{0,2,1:T(8,128)(2,1)S(1)} %slice.39, f32[4,512,512]{1,2,0:T(8,128)S(1)} %get-tuple-element.12, f32[4,512]{1,0:T(4,128)S(1)} %get-tuple-element.11, f32[4,512]{1,0:T(4,128)S(1)} %get-tuple-element.7, pred[512,512]{0,1:T(8,128)(4,1)S(1)} %iota_compare_fusion.1, f32[512,4]{0,1:T(4,128)S(1)} %bitcast.100), kind=kOutput, calls=%fused_computation.21 | convolution fusion | flops 139722752 | bytes 5005312 | tf_op jit(solution)/shard_map/hqk,khd->qhd/dot_general | solution.py:31
  95.1 0.0 copy-done.4
  95.1 2.2 %fusion.2 = (f32[4,512]{1,0:T(4,128)S(1)}, f32[4,512,1024]{2,1,0:T(8,128)S(1)}) fusion(f32[4,1024]{1,0:T(4,128)S(1)} %bitcast.95, f32[4,512]{1,0:T(4,128)S(1)} %get-tuple-element.8, pred[512,1024]{1,0:T(8,128)(4,1)S(1)} %iota_compare_fusion, bf16[512,4,64]{0,2,1:T(8,128)(2,1)S(1)} %copy-done.5, bf16[1024,4,64]{0,2,1:T(8,128)(2,1)S(1)} %copy-done.4), kind=kOutput, calls=%fused_computation.4 | convolution fusion | flops 276822016 | bytes 9732096 | tf_op jit(solution)/shard_map/qhd,khd->hqk/dot_general | solution.py:16
  97.3 2.8 %fusion = f32[4,512]{1,0:T(4,128)S(1)} fusion(f32[4,512,1024]{2,1,0:T(8,128)S(1)} %get-tuple-element.10, f32[4,512]{1,0:T(4,128)S(1)} %get-tuple-element.9, f32[4,1024]{1,0:T(4,128)S(1)} %bitcast.96, f32[4,512]{1,0:T(4,128)S(1)} %get-tuple-element.8, pred[512,1024]{1,0:T(8,128)(4,1)S(1)} %iota_compare_fusion), kind=kLoop, calls=%fused_computation.2 | loop fusion | flops 10483712 | bytes 8953856 | tf_op jit(solution)/shard_map/reduce_sum | solution.py:29
  100.1 2.8 %fusion.28 = bf16[512,4,64]{0,2,1:T(8,128)(2,1)S(1)} fusion(bf16[1024,4,64]{0,2,1:T(8,128)(2,1)S(1)} %reshape_squeeze.8, f32[4,512,1024]{2,1,0:T(8,128)S(1)} %get-tuple-element.10, f32[4,512]{1,0:T(4,128)S(1)} %get-tuple-element.9, f32[4,1024]{1,0:T(4,128)S(1)} %bitcast.97, f32[4,512]{1,0:T(4,128)S(1)} %get-tuple-element.8, ...), kind=kOutput, calls=%fused_computation.23 | convolution fusion | flops 279183360 | bytes 9740288 | tf_op jit(solution)/shard_map/hqk,khd->qhd/dot_general | solution.py:31
  102.9 0.1 pad_maximum_fusion
  103.0 1.1 copy.41
  104.1 3.8 %reduce.3 = bf16[1024,256]{1,0:T(8,128)(2,1)S(1)} reduce(bf16[1024,1,256]{2,1,0:T(2,128)(2,1)S(1)} %bitcast.84, bf16[]{:T(256)} %broadcast.36), dimensions={1}, to_apply=%bitcast.68.reduce_sub_computation | reduce | bytes 1048578
  107.9 0.1 reshape.72
  108.0 17.2 %all_to_all.75 = bf16[8,2,16384]{2,1,0:T(2,128)(2,1)S(1)} all-to-all(bf16[8,2,16384]{2,1,0:T(2,128)(2,1)S(1)} %reshape.72), channel_id=1, replica_groups=mesh['sp'=8,'dp'=4] {'sp'}, dimensions={0} | all-to-all | bytes 1048576 | tf_op jit(solution)/shard_map/all_to_all | solution.py:52
  125.2 0.5 reshape.73
  125.8 0.1 copy.47
  125.9 0.3 copy.42
  126.1 0.0 all-gather.2.cloned.1.call-done
  126.2 5.5 %fusion.9 = bf16[1,128,2048]{2,1,0:T(8,128)(2,1)} fusion(bf16[128,2048]{0,1:T(8,128)(2,1)S(1)} %bitcast.78, bf16[2048,2048]{1,0:T(8,128)(2,1)} %all-gather.2.cloned.1.call-done), kind=kOutput, calls=%fused_computation.13 | convolution fusion | flops 1074003968 | bytes 9437184 | tf_op jit(solution)/shard_map/dot_general | solution.py:54
  (9 shorter events, 0.1 us)
Async XLA Ops:
  6.5 29.5 %copy-start.2 = (bf16[1,128,2048]{2,1,0:T(8,128)(2,1)S(1)}, bf16[1,128,2048]{2,1,0:T(8,128)(2,1)}, u32[]{:S(2)}) copy-start(bf16[1,128,2048]{2,1,0:T(8,128)(2,1)} %param.7) | copy-start | bytes 1572868
  6.5 119.6 %all-gather.2.cloned.1.call-start = ((), (), s32[]{:S(2)}) async-start(), calls=%async_computation.5 | async-start | bytes 10485760 | tf_op jit(solution)/shard_map/all_gather | solution.py:56
  7.3 22.8 %all-to-all-start.2 = ((f32[1,128,32]{1,0,2:T(1,128)}), f32[1,128,32]{1,0,2:T(1,128)S(1)}, u32[]{:S(2)}, u32[]{:S(2)}) async-start(f32[1,128,32]{1,0,2:T(1,128)} %bitcast.98), calls=%async_computation.2 | async-start | bytes 32768 | tf_op jit(solution)/shard_map/all_to_all | solution.py:45
  17.5 37.7 %copy-start.3 = (bf16[1,128,2048]{2,1,0:T(8,128)(2,1)S(1)}, bf16[1,128,2048]{2,1,0:T(8,128)(2,1)}, u32[]{:S(2)}) copy-start(bf16[1,128,2048]{2,1,0:T(8,128)(2,1)} %param.5) | copy-start | bytes 1572868
  30.0 20.0 %all-to-all-start.1 = ((bf16[8,2,16384]{2,1,0:T(2,128)(2,1)}), bf16[8,2,16384]{2,1,0:T(2,128)(2,1)S(1)}, u32[]{:S(2)}, u32[]{:S(2)}) async-start(bf16[8,2,16384]{2,1,0:T(2,128)(2,1)} %reshape.70), calls=%async_computation.1 | async-start | bytes 1048576 | tf_op jit(solution)/shard_map/all_to_all | solution.py:42
  50.0 18.6 %all-to-all-start.3 = ((bf16[8,2,16384]{2,1,0:T(2,128)(2,1)}), bf16[8,2,16384]{2,1,0:T(2,128)(2,1)S(1)}, u32[]{:S(2)}, u32[]{:S(2)}) async-start(bf16[8,2,16384]{2,1,0:T(2,128)(2,1)} %reshape.66), calls=%async_computation.3 | async-start | bytes 1048576 | tf_op jit(solution)/shard_map/all_to_all | solution.py:43
  68.6 18.7 %all-to-all-start = ((bf16[8,2,16384]{2,1,0:T(2,128)(2,1)}), bf16[8,2,16384]{2,1,0:T(2,128)(2,1)S(1)}, u32[]{:S(2)}, u32[]{:S(2)}) async-start(bf16[8,2,16384]{2,1,0:T(2,128)(2,1)} %reshape.68), calls=%async_computation | async-start | bytes 1048576 | tf_op jit(solution)/shard_map/all_to_all | solution.py:41
  87.8 2.7 %copy-start = (bf16[1,4,128,256]{2,3,1,0:T(8,128)(2,1)S(1)}, bf16[1,4,128,256]{2,3,1,0:T(8,128)(2,1)}, u32[]{:S(2)}) copy-start(bf16[1,4,128,256]{2,3,1,0:T(8,128)(2,1)} %slice.45) | copy-start | bytes 786436
  87.8 3.1 %copy-start.1 = (bf16[1,4,128,256]{2,3,1,0:T(8,128)(2,1)S(1)}, bf16[1,4,128,256]{2,3,1,0:T(8,128)(2,1)}, u32[]{:S(2)}) copy-start(bf16[1,4,128,256]{2,3,1,0:T(8,128)(2,1)} %slice.43) | copy-start | bytes 786436
  93.6 1.5 %copy-start.4 = (bf16[1024,4,64]{0,2,1:T(8,128)(2,1)S(1)}, bf16[1024,4,64]{0,2,1:T(8,128)(2,1)}, u32[]{:S(2)}) copy-start(bf16[1024,4,64]{0,2,1:T(8,128)(2,1)} %reshape_squeeze.7) | copy-start | bytes 1572868
  93.6 1.5 %copy-start.5 = (bf16[512,4,64]{0,2,1:T(8,128)(2,1)S(1)}, bf16[512,4,64]{0,2,1:T(8,128)(2,1)}, u32[]{:S(2)}) copy-start(bf16[512,4,64]{0,2,1:T(8,128)(2,1)} %mul.15) | copy-start | bytes 786436
Sparse Core Ops, SparseCore 0:
  8.9 60.9 all-gather.1
where the time goes:
time: 139 us; the launch traced here: 138 us
  other arithmetic  43 us (31%)
  starting transfers between devices  24.4 us (18%)
  blocking collectives  17.2 us (12%)
  local copies, waits for them, and re-layouts  16.5 us (12%)
  between operations  13.7 us (10%)
  matrix products  13.1 us (9%)
  waiting for transfers between devices  10.5 us (8%)
    unnamed x4, other arithmetic  38.4 us
    all_to_all x1, blocking collectives, local(): lax.all_to_all(attended, 'sp', split_axis=1, concat_axis=2, tiled=True)  17.2 us
    unnamed x28, local copies, waits for them, and re-layouts  9.83 us
    all_to_all x1, waiting for transfers between devices, local(): lax.all_to_all(queries, 'sp', split_axis=2, concat_axis=1, tiled=True)  8.91 us
    all_to_all x1, starting transfers between devices, local(): lax.all_to_all(gate_totals, 'sp', split_axis=2, concat_axis=1, tiled=True)  7.29 us
    all_to_all x1, starting transfers between devices, local(): lax.all_to_all(keys, 'sp', split_axis=2, concat_axis=1, tiled=True)  6 us
    all_to_all x1, starting transfers between devices, local(): lax.all_to_all(queries, 'sp', split_axis=2, concat_axis=1, tiled=True)  5.88 us
    dot_general x1, matrix products, local(): jnp.dot(flat_rows, lax.all_gather(w_out, 'dp', axis=1, tiled=True), prefe...  5.46 us
  transfers between devices with their start and end apart: 5, of which 3 were waited for; matrix products, arithmetic and copies ran while one was open for 48% of the time, Pallas kernels for 0%

commit v1 on v0

--- a/solution.py
+++ b/solution.py
@@ -4,6 +4,15 @@
 from jax.sharding import PartitionSpec as P
 
 HEAD_DIM = 64
+
+
+def _resolve_group(original, chip_axis):
+    oldest = lax.axis_size(chip_axis)
+    outer = jnp.split(original, oldest, 2)
+    built = jnp.stack(outer, 0)
+    q_next = lax.all_to_all(built, axis_name=chip_axis, concat_axis=0, split_axis=0)
+    field_out = jnp.concatenate(q_next, 1)
+    return field_out
 
 
 def attend(queries, key_rows, value_rows, totals):
@@ -38,7 +47,7 @@
 
 def local(queries, keys, values, gate_totals, w_out):
     moved = (
-        lax.all_to_all(queries, "sp", split_axis=2, concat_axis=1, tiled=True),
+        _resolve_group(queries, "sp"),
         lax.all_to_all(keys, "sp", split_axis=2, concat_axis=1, tiled=True),
         lax.all_to_all(values, "sp", split_axis=2, concat_axis=1, tiled=True),
     )

time: 139 us -> 138 us (level)
  other arithmetic: 43 us -> 31.4 us
  waiting for transfers between devices: 10.5 us -> 20.6 us
  local copies, waits for them, and re-layouts: 16.5 us -> 18.4 us
  starting transfers between devices: 24.4 us -> 23 us
    unnamed x4 -> x3, other arithmetic: 38.4 us -> 26.8 us
    all_to_all x1, waiting for transfers between devices: 0.11 us -> 10.2 us  [local(): lax.all_to_all(values, 'sp', split_axis=2, concat_axis=1, tiled=True)]
    all_to_all x1, starting transfers between devices: 5.88 us -> 3.68 us  [_resolve_group(): lax.all_to_all(built, axis_name=chip_axis, concat_axis=0, split_axis=0)]
    unnamed x28 -> x29, local copies, waits for them, and re-layouts: 9.83 us -> 11.9 us
  transfers between devices with their start and end apart: 5 -> 5, of which waited for: 3 -> 2; matrix products, arithmetic and copies ran while one was open for 48% -> 42% of each run, Pallas kernels for 0% -> 0%
where the time goes in v1:
time: 138 us
  other arithmetic  31.4 us (23%)
  starting transfers between devices  23 us (17%)
  waiting for transfers between devices  20.6 us (15%)
  local copies, waits for them, and re-layouts  18.4 us (13%)
  blocking collectives  17.5 us (13%)
  between operations  13.7 us (10%)
  matrix products  13.1 us (9%)
    unnamed x3, other arithmetic  26.8 us
    all_to_all x1, blocking collectives, local(): lax.all_to_all(attended, 'sp', split_axis=1, concat_axis=2, tiled=True)  17.5 us
    unnamed x29, local copies, waits for them, and re-layouts  11.9 us
    all_to_all x1, waiting for transfers between devices, local(): lax.all_to_all(values, 'sp', split_axis=2, concat_axis=1, tiled=True)  10.2 us
    all_to_all x1, waiting for transfers between devices, _resolve_group(): lax.all_to_all(built, axis_name=chip_axis, concat_axis=0, split_axis=0)  9.62 us
    all_to_all x1, starting transfers between devices, local(): lax.all_to_all(gate_totals, 'sp', split_axis=2, concat_axis=1, tiled=True)  7.29 us
    all_to_all x1, starting transfers between devices, local(): lax.all_to_all(keys, 'sp', split_axis=2, concat_axis=1, tiled=True)  6 us
    all_to_all x1, starting transfers between devices, local(): lax.all_to_all(values, 'sp', split_axis=2, concat_axis=1, tiled=True)  5.99 us
  transfers between devices with their start and end apart: 5, of which 2 were waited for; matrix products, arithmetic and copies ran while one was open for 42% of the time, Pallas kernels for 0%

profile of v1, /device:TPU:0, one launch (start us, length us, event | category | flops | bytes accessed | tf_op | source)
XLA Modules:
  0.0 137.8 jit_solution(782201972838408311)
XLA Ops:
  6.5 0.0 all-gather.2.cloned.1.call-start
  6.5 0.7 all-gather.2.cloned.1.call-update
  7.3 7.3 %all-to-all-start.2 = ((f32[1,128,32]{1,0,2:T(1,128)}), f32[1,128,32]{1,0,2:T(1,128)S(1)}, u32[]{:S(2)}, u32[]{:S(2)}) async-start(f32[1,128,32]{1,0,2:T(1,128)} %bitcast.106), calls=%async_computation.2 | async-start | bytes 32768 | tf_op jit(solution)/shard_map/all_to_all | solution.py:54
  14.6 2.3 %copy.34 = bf16[1,128,2048]{1,0,2:T(2,128)(2,1)S(1)} copy(bf16[1,128,2048]{2,1,0:T(8,128)(2,1)} %param.6) | data formatting | bytes 1048576 | tf_op args[1]
  16.9 0.0 copy-start.2
  16.9 0.6 broadcast.36
  17.5 11.5 %reduce.1 = bf16[2048,128]{1,0:T(8,128)(2,1)S(1)} reduce(bf16[2048,1,128]{2,1,0:T(2,128)(2,1)S(1)} %bitcast.93, bf16[]{:T(256)} %broadcast.36), dimensions={1}, to_apply=%bitcast.77.reduce_sub_computation | reduce | bytes 1048578
  29.0 1.0 reshape.67
  30.0 0.0 all-to-all-done.2
  30.0 6.0 %all-to-all-start.1 = ((bf16[8,2,16384]{2,1,0:T(2,128)(2,1)}), bf16[8,2,16384]{2,1,0:T(2,128)(2,1)S(1)}, u32[]{:S(2)}, u32[]{:S(2)}) async-start(bf16[8,2,16384]{2,1,0:T(2,128)(2,1)} %reshape.67), calls=%async_computation.1 | async-start | bytes 1048576 | tf_op jit(solution)/shard_map/all_to_all | solution.py:51
  36.0 0.0 copy-done.1
  36.0 0.8 copy.37
  36.7 11.5 %reduce = bf16[2048,128]{1,0:T(8,128)(2,1)S(1)} reduce(bf16[2048,1,128]{2,1,0:T(2,128)(2,1)S(1)} %bitcast.95, bf16[]{:T(256)} %broadcast.36), dimensions={1}, to_apply=%bitcast.75.reduce_sub_computation | reduce | bytes 1048578
  48.2 0.9 reshape.65
  49.2 0.6 bitcast_dynamic-update-slice_fusion.7
  49.8 0.6 bitcast_dynamic-update-slice_fusion.6
  50.4 0.6 bitcast_dynamic-update-slice_fusion.5
  51.0 0.0 all-to-all-done.1
  51.0 6.0 %all-to-all-start.3 = ((bf16[8,2,16384]{2,1,0:T(2,128)(2,1)}), bf16[8,2,16384]{2,1,0:T(2,128)(2,1)S(1)}, u32[]{:S(2)}, u32[]{:S(2)}) async-start(bf16[8,2,16384]{2,1,0:T(2,128)(2,1)} %reshape.65), calls=%async_computation.3 | async-start | bytes 1048576 | tf_op jit(solution)/shard_map/all_to_all | solution.py:52
  57.0 0.6 bitcast_dynamic-update-slice_fusion.4
  57.7 0.6 bitcast_dynamic-update-slice_fusion.3
  58.3 0.6 bitcast_dynamic-update-slice_fusion.2
  58.9 0.6 bitcast_dynamic-update-slice_fusion.1
  59.5 0.6 bitcast_dynamic-update-slice_fusion
  60.2 10.2 %all-to-all-done.3 = bf16[8,2,16384]{2,1,0:T(2,128)(2,1)S(1)} async-done(((bf16[8,2,16384]{2,1,0:T(2,128)(2,1)}), bf16[8,2,16384]{2,1,0:T(2,128)(2,1)S(1)}, u32[]{:S(2)}, u32[]{:S(2)}) %all-to-all-start.3) | async-done | bytes 524320 | tf_op jit(solution)/shard_map/all_to_all | solution.py:52
  70.4 3.7 %all-to-all-start = ((bf16[8,1,128,256]{3,2,1,0:T(8,128)(2,1)}), bf16[8,1,128,256]{3,2,1,0:T(8,128)(2,1)S(1)}, u32[]{:S(2)}, u32[]{:S(2)}) async-start(bf16[8,1,128,256]{3,2,1,0:T(8,128)(2,1)} %bitcast_dynamic-update-slice_fusion), calls=%async_computation | async-start | bytes 1048576 | tf_op jit(solution)/shard_map/all_to_all | solution.py:13
  74.1 0.1 iota_compare_fusion.1
  74.2 0.4 iota_compare_fusion
  74.6 0.5 reshape.68
  75.1 0.1 copy.47
  75.2 0.3 copy.41
  75.5 0.7 slice.45
  76.3 0.5 reshape.66
  76.8 0.1 copy.46
  76.9 0.3 copy.42
  77.3 1.0 reshape_squeeze.6
  78.3 9.6 %all-to-all-done = bf16[8,1,128,256]{3,2,1,0:T(8,128)(2,1)S(1)} async-done(((bf16[8,1,128,256]{3,2,1,0:T(8,128)(2,1)}), bf16[8,1,128,256]{3,2,1,0:T(8,128)(2,1)S(1)}, u32[]{:S(2)}, u32[]{:S(2)}) %all-to-all-start) | async-done | bytes 524320 | tf_op jit(solution)/shard_map/all_to_all | solution.py:13
  87.9 0.2 copy.40
  88.1 0.8 mul.15
  88.9 0.2 reshape_squeeze.7
  89.2 0.0 copy-done
  89.2 0.2 copy.35
  89.4 0.1 slice.35
  89.5 0.2 copy.33
  89.7 0.1 mul.13
  89.8 0.2 copy.38
  90.0 0.1 slice.39
  90.1 1.2 fusion.8
  91.3 1.2 fusion.6
  92.5 0.0 copy-start.3
  92.6 1.4 %fusion.22 = bf16[512,4,64]{0,2,1:T(8,128)(2,1)S(1)} fusion(bf16[512,4,64]{0,2,1:T(8,128)(2,1)S(1)} %slice.39, f32[4,512,512]{1,2,0:T(8,128)S(1)} %get-tuple-element.12, f32[4,512]{1,0:T(4,128)S(1)} %get-tuple-element.11, f32[4,512]{1,0:T(4,128)S(1)} %get-tuple-element.7, pred[512,512]{0,1:T(8,128)(4,1)S(1)} %iota_compare_fusion.1, f32[512,4]{0,1:T(4,128)S(1)} %bitcast.108), kind=kOutput, calls=%fused_computation.21 | convolution fusion | flops 139722752 | bytes 5005312 | tf_op jit(solution)/shard_map/hqk,khd->qhd/dot_general | solution.py:40
  94.0 2.3 %fusion.2 = (f32[4,512]{1,0:T(4,128)S(1)}, f32[4,512,1024]{2,1,0:T(8,128)S(1)}) fusion(f32[4,1024]{1,0:T(4,128)S(1)} %bitcast.103, f32[4,512]{1,0:T(4,128)S(1)} %get-tuple-element.8, pred[512,1024]{1,0:T(8,128)(4,1)S(1)} %iota_compare_fusion, bf16[512,4,64]{0,2,1:T(8,128)(2,1)S(1)} %copy-done.4, bf16[1024,4,64]{0,2,1:T(8,128)(2,1)S(1)} %copy-done.3), kind=kOutput, calls=%fused_computation.4 | convolution fusion | flops 276822016 | bytes 9732096 | tf_op jit(solution)/shard_map/qhd,khd->hqk/dot_general | solution.py:25
  96.3 2.8 %fusion = f32[4,512]{1,0:T(4,128)S(1)} fusion(f32[4,512,1024]{2,1,0:T(8,128)S(1)} %get-tuple-element.10, f32[4,512]{1,0:T(4,128)S(1)} %get-tuple-element.9, f32[4,1024]{1,0:T(4,128)S(1)} %bitcast.104, f32[4,512]{1,0:T(4,128)S(1)} %get-tuple-element.8, pred[512,1024]{1,0:T(8,128)(4,1)S(1)} %iota_compare_fusion), kind=kLoop, calls=%fused_computation.2 | loop fusion | flops 10483712 | bytes 8953856 | tf_op jit(solution)/shard_map/reduce_sum | solution.py:38
  99.1 2.8 %fusion.28 = bf16[512,4,64]{0,2,1:T(8,128)(2,1)S(1)} fusion(bf16[1024,4,64]{0,2,1:T(8,128)(2,1)S(1)} %reshape_squeeze.7, f32[4,512,1024]{2,1,0:T(8,128)S(1)} %get-tuple-element.10, f32[4,512]{1,0:T(4,128)S(1)} %get-tuple-element.9, f32[4,1024]{1,0:T(4,128)S(1)} %bitcast.105, f32[4,512]{1,0:T(4,128)S(1)} %get-tuple-element.8, ...), kind=kOutput, calls=%fused_computation.23 | convolution fusion | flops 279183360 | bytes 9740288 | tf_op jit(solution)/shard_map/hqk,khd->qhd/dot_general | solution.py:40
  101.9 0.1 pad_maximum_fusion
  102.0 1.1 copy.43
  103.0 3.8 %reduce.2 = bf16[1024,256]{1,0:T(8,128)(2,1)S(1)} reduce(bf16[1024,1,256]{2,1,0:T(2,128)(2,1)S(1)} %bitcast.94, bf16[]{:T(256)} %broadcast.36), dimensions={1}, to_apply=%bitcast.79.reduce_sub_computation | reduce | bytes 1048578
  106.9 0.1 reshape.69
  107.0 17.5 %all_to_all.65 = bf16[8,2,16384]{2,1,0:T(2,128)(2,1)S(1)} all-to-all(bf16[8,2,16384]{2,1,0:T(2,128)(2,1)S(1)} %reshape.69), channel_id=1, replica_groups=mesh['sp'=8,'dp'=4] {'sp'}, dimensions={0} | all-to-all | bytes 1048576 | tf_op jit(solution)/shard_map/all_to_all | solution.py:61
  124.5 0.5 reshape.70
  125.1 0.1 copy.48
  125.2 0.3 copy.44
  125.4 0.0 all-gather.2.cloned.1.call-done
  125.5 5.5 %fusion.9 = bf16[1,128,2048]{2,1,0:T(8,128)(2,1)} fusion(bf16[128,2048]{0,1:T(8,128)(2,1)S(1)} %bitcast.89, bf16[2048,2048]{1,0:T(8,128)(2,1)} %all-gather.2.cloned.1.call-done), kind=kOutput, calls=%fused_computation.13 | convolution fusion | flops 1074003968 | bytes 9437184 | tf_op jit(solution)/shard_map/dot_general | solution.py:63
  (10 shorter events, 0.1 us)
Async XLA Ops:
  6.5 29.4 %copy-start.1 = (bf16[1,128,2048]{2,1,0:T(8,128)(2,1)S(1)}, bf16[1,128,2048]{2,1,0:T(8,128)(2,1)}, u32[]{:S(2)}) copy-start(bf16[1,128,2048]{2,1,0:T(8,128)(2,1)} %param.7) | copy-start | bytes 1572868
  6.5 118.9 %all-gather.2.cloned.1.call-start = ((), (), s32[]{:S(2)}) async-start(), calls=%async_computation.5 | async-start | bytes 10485760 | tf_op jit(solution)/shard_map/all_gather | solution.py:65
  7.3 22.7 %all-to-all-start.2 = ((f32[1,128,32]{1,0,2:T(1,128)}), f32[1,128,32]{1,0,2:T(1,128)S(1)}, u32[]{:S(2)}, u32[]{:S(2)}) async-start(f32[1,128,32]{1,0,2:T(1,128)} %bitcast.106), calls=%async_computation.2 | async-start | bytes 32768 | tf_op jit(solution)/shard_map/all_to_all | solution.py:54
  16.9 32.3 %copy-start.2 = (bf16[1,128,2048]{2,1,0:T(8,128)(2,1)S(1)}, bf16[1,128,2048]{2,1,0:T(8,128)(2,1)}, u32[]{:S(2)}) copy-start(bf16[1,128,2048]{2,1,0:T(8,128)(2,1)} %param.5) | copy-start | bytes 1572868
  30.0 21.1 %all-to-all-start.1 = ((bf16[8,2,16384]{2,1,0:T(2,128)(2,1)}), bf16[8,2,16384]{2,1,0:T(2,128)(2,1)S(1)}, u32[]{:S(2)}, u32[]{:S(2)}) async-start(bf16[8,2,16384]{2,1,0:T(2,128)(2,1)} %reshape.67), calls=%async_computation.1 | async-start | bytes 1048576 | tf_op jit(solution)/shard_map/all_to_all | solution.py:51
  51.0 19.4 %all-to-all-start.3 = ((bf16[8,2,16384]{2,1,0:T(2,128)(2,1)}), bf16[8,2,16384]{2,1,0:T(2,128)(2,1)S(1)}, u32[]{:S(2)}, u32[]{:S(2)}) async-start(bf16[8,2,16384]{2,1,0:T(2,128)(2,1)} %reshape.65), calls=%async_computation.3 | async-start | bytes 1048576 | tf_op jit(solution)/shard_map/all_to_all | solution.py:52
  70.4 17.5 %all-to-all-start = ((bf16[8,1,128,256]{3,2,1,0:T(8,128)(2,1)}), bf16[8,1,128,256]{3,2,1,0:T(8,128)(2,1)S(1)}, u32[]{:S(2)}, u32[]{:S(2)}) async-start(bf16[8,1,128,256]{3,2,1,0:T(8,128)(2,1)} %bitcast_dynamic-update-slice_fusion), calls=%async_computation | async-start | bytes 1048576 | tf_op jit(solution)/shard_map/all_to_all | solution.py:13
  76.8 12.4 %copy-start = (bf16[1,4,128,256]{2,3,1,0:T(8,128)(2,1)S(1)}, bf16[1,4,128,256]{2,3,1,0:T(8,128)(2,1)}, u32[]{:S(2)}) copy-start(bf16[1,4,128,256]{2,3,1,0:T(8,128)(2,1)} %slice.45) | copy-start | bytes 786436
  92.5 1.5 %copy-start.3 = (bf16[1024,4,64]{0,2,1:T(8,128)(2,1)S(1)}, bf16[1024,4,64]{0,2,1:T(8,128)(2,1)}, u32[]{:S(2)}) copy-start(bf16[1024,4,64]{0,2,1:T(8,128)(2,1)} %reshape_squeeze.6) | copy-start | bytes 1572868
  92.5 1.5 %copy-start.4 = (bf16[512,4,64]{0,2,1:T(8,128)(2,1)S(1)}, bf16[512,4,64]{0,2,1:T(8,128)(2,1)}, u32[]{:S(2)}) copy-start(bf16[512,4,64]{0,2,1:T(8,128)(2,1)} %mul.15) | copy-start | bytes 786436
Sparse Core Ops, SparseCore 0:
  8.9 60.9 all-gather.1
